TPU v7x, 512 devices: a 4x2x32 block of a 4x8x32 slice. The times are simulated.
512 devices in a mesh: grp: 2 (over y), sp: 64 (over z, core), tp: 4 (over x).
Axes of the slice: x: 4, y: 2, z: 32, core: 2. Of those that a mesh axis runs over, the one named last changes fastest.
The devices are a block of a 4x8x32 slice.
Arguments:
- tokens: bfloat16 [131072, 2048], P(('grp', 'sp', 'tp')), parts along dimension 0, may hold values from -6 to 6
- step: float32 [131072], P(('grp', 'sp')), parts along dimension 0, may hold values from 0.2 to 3.75
- in_gain: float32 [2048], replicated, may hold values from 0.1 to 1.9
- in_proj: bfloat16 [2048, 512], P(None, 'tp'), may hold values from -0.125 to 0.125
- decay_rate: float32 [32, 64], P('tp'), may hold values from 1.5258789e-06 to 0.04
- frequency: float32 [32, 64], P('tp'), may hold values from 0.2 to 3
- input_map: float32 [2, 32, 64, 16], P(None, 'tp'), may hold values from -1 to 1
- readout: float32 [2, 32, 16, 64], P(None, 'tp'), may hold values from -0.75 to 0.75
- out_gain: float32 [512], replicated, may hold values from 0.1 to 1.9
- out_proj: bfloat16 [512, 2048], replicated, may hold values from -0.25 to 0.25
Outputs:
- mixed: bfloat16 [131072, 2048], P(('grp', 'sp', 'tp')), parts along dimension 0
There are 2 independent parts, one for each index of `grp`. A program takes and returns all parts, laid end to end along the dimension named above; an argument that names none is the same for every part. Nothing has to cross between parts.
All inputs are finite; a program needn't handle non-finite values.
Results may differ from a plain program's by a relative error of at most 0.01.
Values may be sent and summed in bfloat16 or wider, within the bound.
No kernel may reach another device: no remote copies, remote signals or barrier semaphores. Data moves between devices by JAX's collectives and lax.ppermute only.
A program may use at most 64 MiB of HBM per device.

v0:
```python
from functools import partial
import jax
import jax.numpy as jnp
from jax import lax
from jax.sharding import PartitionSpec as P

SPAN = 64
HIGHEST = lax.Precision.HIGHEST


def gathered_once(array, axis):
    leaves = jax.tree.leaves(array)
    sequence = sorted(range(len(leaves)), key=lambda k: -leaves[k].size)
    width = (1, *leaves[sequence[0]].shape)[-1]
    lines = [
        jnp.pad(leaves[k].reshape(-1), (0, -leaves[k].size % width)).reshape(-1, width)
        for k in sequence
    ]
    both, at, found = (lax.all_gather(jnp.concatenate(lines), axis), 0, {})
    for k, line in zip(sequence, lines):
        section = both[:, at : at + len(line)].reshape(len(both), -1)
        found[k] = section[:, : leaves[k].size].reshape(-1, *leaves[k].shape)
        at += len(line)
    numbers = iter(range(len(leaves)))
    return jax.tree.map(lambda _: found[next(numbers)], array)


def entering(value, axis, join, neutral):
    count, mine = (lax.axis_size(axis), lax.axis_index(axis))
    pieces = gathered_once(value, axis)
    so_far = jax.tree.map(
        lambda part, zero: jnp.full_like(part, 0) + jnp.asarray(zero, part.dtype), value, neutral
    )

    def lap(position, so_far):
        longer = join(so_far, jax.tree.map(lambda part: part[position], pieces))
        return jax.tree.map(lambda new, old: jnp.where(position < mine, new, old), longer, so_far)

    return lax.fori_loop(0, count - 1, lap, so_far)


def compose(earlier, later):
    a_re, a_im, b_re, b_im = earlier
    c_re, c_im, d_re, d_im = later
    return (
        c_re * a_re - c_im * a_im,
        c_re * a_im + c_im * a_re,
        c_re * b_re - c_im * b_im + d_re,
        c_re * b_im + c_im * b_re + d_im,
    )


def rms_rows(values, gain):
    values = values.astype(jnp.float32)
    scaled = values * lax.rsqrt(jnp.mean(values * values, axis=-1, keepdims=True) + 1e-06)
    return (scaled * gain).astype(jnp.bfloat16)


def block_tables(input_map, readout):
    groups = input_map.shape[1]
    unit = jnp.eye(groups, dtype=jnp.float32)
    push_re = jnp.einsum("gph,gk->ghkp", input_map[0], unit, precision=HIGHEST)
    push_im = jnp.einsum("gph,gk->ghkp", input_map[1], unit, precision=HIGHEST)
    read_re = jnp.einsum("ghp,gk->gpkh", readout[0], unit, precision=HIGHEST)
    read_im = jnp.einsum("ghp,gk->gpkh", readout[1], unit, precision=HIGHEST)
    inner = push_re.shape[0] * push_re.shape[1]
    flat = push_re.shape[2] * push_re.shape[3]
    return (
        push_re.reshape(inner, flat),
        push_im.reshape(inner, flat),
        read_re.reshape(flat, inner),
        read_im.reshape(flat, inner),
    )


def response(s_re, s_im, read_re, read_im):
    value = jnp.dot(s_re, read_re, precision=HIGHEST) - jnp.dot(s_im, read_im, precision=HIGHEST)
    return jax.nn.gelu(value, approximate=True).astype(jnp.bfloat16)


def advance(carry, piece, rates, freqs, tables, lower, keep):
    drive_part, time_part = piece
    push_re, push_im, read_re, read_im = tables
    own = time_part[:, None]
    magnitude = jnp.exp(-rates[None] * own)
    a_re = magnitude * jnp.cos(freqs[None] * own)
    a_im = magnitude * jnp.sin(freqs[None] * own)
    lam_re = -rates
    denom = lam_re * lam_re + freqs * freqs
    n_re = a_re - 1.0
    z_re = (n_re * lam_re + a_im * freqs) / denom
    z_im = (a_im * lam_re - n_re * freqs) / denom
    grouped = drive_part.astype(jnp.float32)
    in_re = jnp.dot(grouped, push_re, precision=HIGHEST)
    in_im = jnp.dot(grouped, push_im, precision=HIGHEST)
    i_re = z_re * in_re - z_im * in_im
    i_im = z_re * in_im + z_im * in_re
    elapsed = jnp.dot(lower, time_part, precision=HIGHEST)[:, None]
    grow = jnp.exp(rates[None] * elapsed)
    angle = freqs[None] * elapsed
    cosine = jnp.cos(angle)
    sine = jnp.sin(angle)
    w_re = grow * (cosine * i_re + sine * i_im)
    w_im = grow * (cosine * i_im - sine * i_re)
    acc_re = jnp.dot(lower, w_re, precision=HIGHEST)
    acc_im = jnp.dot(lower, w_im, precision=HIGHEST)
    shrink = jnp.exp(-rates[None] * elapsed)
    c_re = shrink * cosine
    c_im = shrink * sine
    s_re = c_re * acc_re - c_im * acc_im
    s_im = c_re * acc_im + c_im * acc_re
    d_re, d_im, e_re, e_im = carry
    full_re = s_re + c_re * e_re - c_im * e_im
    full_im = s_im + c_re * e_im + c_im * e_re
    cum_re = c_re * d_re - c_im * d_im
    cum_im = c_re * d_im + c_im * d_re
    ends = (cum_re[-1], cum_im[-1], full_re[-1], full_im[-1])
    return (ends, (cum_re, cum_im, full_re, full_im))


def on_device(
    tokens, step, in_gain, in_proj, decay_rate, frequency, input_map, readout, out_gain, out_proj
):
    normed = rms_rows(tokens, in_gain)
    rates, freqs, maps, reads = (decay_rate, frequency, input_map, readout)
    drive = jnp.dot(
        lax.all_gather(normed, "tp", axis=0, tiled=True),
        in_proj,
        preferred_element_type=jnp.float32,
    ).astype(jnp.bfloat16)
    tables = block_tables(maps, reads)
    flat_rates = rates.reshape(-1)
    flat_freqs = freqs.reshape(-1)
    seq_rows = drive.shape[0]
    block_count = seq_rows // SPAN
    drive_blocks = drive.reshape(block_count, SPAN, -1)
    time_blocks = step.reshape(block_count, SPAN)
    rows_index = lax.broadcasted_iota(jnp.int32, (SPAN, SPAN), 0)
    cols_index = lax.broadcasted_iota(jnp.int32, (SPAN, SPAN), 1)
    lower = (cols_index <= rows_index).astype(jnp.float32)
    zeros = jnp.zeros(flat_rates.shape, jnp.float32)
    ones = jnp.ones(flat_rates.shape, jnp.float32)
    start_carry = (ones, zeros, zeros, zeros)
    keep_first = "states"
    ends, stored = lax.scan(
        partial(
            advance, rates=flat_rates, freqs=flat_freqs, tables=tables, lower=lower, keep=keep_first
        ),
        start_carry,
        (drive_blocks, time_blocks),
    )
    incoming = entering(ends, "sp", compose, start_carry)
    cum_re, cum_im, full_re, full_im = stored
    width = flat_rates.shape[0]
    cum_re = cum_re.reshape(seq_rows, width)
    cum_im = cum_im.reshape(seq_rows, width)
    state_re = full_re.reshape(seq_rows, width) + cum_re * incoming[2] - cum_im * incoming[3]
    state_im = full_im.reshape(seq_rows, width) + cum_re * incoming[3] + cum_im * incoming[2]
    answer = response(state_re, state_im, tables[2], tables[3])
    gathered = lax.all_to_all(answer, "tp", split_axis=0, concat_axis=1, tiled=True)
    shaped = rms_rows(gathered, out_gain)
    return jnp.dot(shaped, out_proj, preferred_element_type=jnp.float32).astype(jnp.bfloat16)


def solution(mesh):
    placed = (
        P(("grp", "sp", "tp"), None),
        P(("grp", "sp")),
        P(),
        P(None, "tp"),
        P("tp", None),
        P("tp", None),
        P(None, "tp", None, None),
        P(None, "tp", None, None),
        P(),
        P(),
    )
    return jax.shard_map(
        on_device,
        mesh=mesh,
        in_specs=placed,
        out_specs=P(("grp", "sp", "tp"), None),
        check_vma=False,
    )
```

profile of v0, /device:TPU:33, one launch (start us, length us, event | category | flops | bytes accessed | tf_op | source)
XLA Modules:
  0.0 373.2 jit_solution(620879934638658215)
XLA Ops:
  8.3 2.5 fusion.46
  15.7 85.1 %all-gather.4.cloned.1.call-done = bf16[1024,2048]{1,0:T(8,128)(2,1)} async-done(((bf16[256,2048]{1,0:T(8,128)(2,1)}), bf16[1024,2048]{1,0:T(8,128)(2,1)}) %all-gather.4.cloned.1.call-update) | async-done | bytes 4194320 | tf_op jit(solution)/shard_map/all_gather | solution.py:127
  100.8 4.3 %convolution_convert_fusion.1 = bf16[1024,128]{1,0:T(8,128)(2,1)} fusion(bf16[1024,2048]{1,0:T(8,128)(2,1)} %all-gather.4.cloned.1.call-done, bf16[2048,128]{1,0:T(8,128)(2,1)} %param.17), kind=kOutput, calls=%fused_computation.81 | convolution fusion | flops 537001984 | bytes 4980736 | tf_op jit(solution)/shard_map/dot_general | solution.py:126
  106.2 173.9 %while.48 = (s32[]{:T(128)}, f32[512]{0:T(512)S(1)}, f32[512]{0:T(512)S(1)}, f32[512]{0:T(512)}, f32[512]{0:T(512)}, /*index=5*/f32[16,64,512]{2,1,0:T(8,128)}, ...) while((s32[]{:T(128)}, f32[512]{0:T(512)S(1)}, ...), condition=%wide.wide.region_2.3_spmd.clone.clone.clone, body=%wide.wide.region_1.2_spmd.clone.clone.clone.sunk | while | flops 153889792 | bytes 4405837 | solution.py:145
  110.2 2.0 convolution_bitcast_fusion.8
  112.3 3.0 add_dynamic-update-slice_fusion.3
  123.2 3.0 add_dynamic-update-slice_fusion.3
  131.9 2.0 convolution_bitcast_fusion.8
  134.1 3.0 add_dynamic-update-slice_fusion.3
  142.8 2.0 convolution_bitcast_fusion.8
  144.9 3.0 add_dynamic-update-slice_fusion.3
  153.7 2.0 convolution_bitcast_fusion.8
  155.8 3.0 add_dynamic-update-slice_fusion.3
  164.6 2.0 convolution_bitcast_fusion.8
  166.7 3.0 add_dynamic-update-slice_fusion.3
  177.6 3.0 add_dynamic-update-slice_fusion.3
  186.3 2.0 convolution_bitcast_fusion.8
  188.4 3.0 add_dynamic-update-slice_fusion.3
  197.2 2.0 convolution_bitcast_fusion.8
  199.3 3.0 add_dynamic-update-slice_fusion.3
  210.2 3.0 add_dynamic-update-slice_fusion.3
  221.0 3.0 add_dynamic-update-slice_fusion.3
  229.8 2.0 convolution_bitcast_fusion.8
  231.9 3.0 add_dynamic-update-slice_fusion.3
  242.8 3.0 add_dynamic-update-slice_fusion.3
  253.6 3.0 add_dynamic-update-slice_fusion.3
  264.5 3.0 add_dynamic-update-slice_fusion.3
  275.4 3.0 add_dynamic-update-slice_fusion.3
  280.9 60.4 %all-gather.1 = f32[64,4,512]{2,1,0:T(4,128)S(1)} all-gather(f32[1,4,512]{2,1,0:T(4,128)S(1)} %maximum_bitcast_fusion), channel_id=2, replica_groups=mesh['grp'=2,'sp'=64,'tp'=4] {'sp'}, dimensions={0}, use_global_device_ids=true | all-gather | bytes 532480 | tf_op jit(solution)/shard_map/all_gather | solution.py:19
  341.7 5.1 %while.47 = (s32[]{:T(128)}, f32[512]{0:T(512)S(1)}, f32[512]{0:T(512)S(1)}, s32[]{:T(128)}, f32[64,512]{1,0:T(8,128)S(1)}, /*index=5*/f32[64,512]{1,0:T(8,128)S...) while((s32[]{:T(128)}, f32[512]{0:T(512)S(1)}, f32[512]{0:T(512)S(1)}, ...), condition=%wide.region_4.5_spmd.clone, body=%wide.region_3.4_spmd.clone.sunk | while | flops 6148 | bytes 32897 | solution.py:39
  346.8 4.6 %multiply_add_fusion.5 = (f32[16,64,512]{2,1,0:T(8,128)S(1)}, f32[16,64,512]{2,1,0:T(8,128)S(1)}) fusion(f32[16,64,512]{2,1,0:T(8,128)} %get-tuple-element.435, f32[16,64,512]{2,1,0:T(8,128)} %get-tuple-element.437, f32[16,64,512]{2,1,0:T(8,128)} %get-tuple-element.429, f32[512]{0:T(512)S(1)} %get-tuple-element.436, f32[512]{0:T(512)S(1)} %get-tuple-element.434, ...), kind=kLoop, calls=%fused_computation.78 | loop fusion | flops 4194304 | bytes 12587008 | tf_op jit(solution)/shard_map/add | solution.py:158
  355.2 9.2 %all_to_all.13 = bf16[4,256,128]{1,2,0:T(8,128)(2,1)S(1)} all-to-all(bf16[4,256,128]{1,2,0:T(8,128)(2,1)S(1)} %copy.20), channel_id=1, replica_groups=mesh['grp'=2,'sp'=64,'tp'=4] {'tp'}, dimensions={0} | all-to-all | bytes 524288 | tf_op jit(solution)/shard_map/all_to_all | solution.py:160
  (627 shorter events, 124.1 us)
Async XLA Ops:
  6.5 358.1 %copy-start = (bf16[512,2048]{1,0:T(8,128)(2,1)S(1)}, bf16[512,2048]{1,0:T(8,128)(2,1)}, u32[]{:S(2)}) copy-start(bf16[512,2048]{1,0:T(8,128)(2,1)} %param.23) | copy-start | bytes 6291460
  6.6 6.4 %copy-start.12 = (f32[1024]{0:T(1024)S(1)}, f32[1024]{0:T(1024)}, u32[]{:S(2)}) copy-start(f32[1024]{0:T(1024)} %param.15) | copy-start | bytes 12292
  6.6 7.0 %copy-start.3 = (f32[2,8,16,64]{3,2,1,0:T(8,128)S(1)}, f32[2,8,16,64]{3,2,1,0:T(8,128)}, u32[]{:S(2)}) copy-start(f32[2,8,16,64]{3,2,1,0:T(8,128)} %param.21) | copy-start | bytes 196612
  6.6 94.2 %all-gather.4.cloned.1.call-start = ((), (), s32[]{:S(2)}) async-start(), calls=%async_computation.1 | async-start | bytes 5242880 | tf_op jit(solution)/shard_map/all_gather | solution.py:127
  128.3 5.7 %copy-start.5 = (f32[1,512]{1,0:T(1,128)S(1)}, f32[1,512]{1,0:T(1,128)}, u32[]{:S(2)}) copy-start(f32[1,512]{1,0:T(1,128)} %get-tuple-element.1028) | copy-start | bytes 6148 | tf_op jit(solution)/shard_map/while
  128.3 5.7 %copy-start.10 = (f32[512]{0:T(512)S(1)}, f32[512]{0:T(512)}, u32[]{:S(2)}) copy-start(f32[512]{0:T(512)} %get-tuple-element.1001) | copy-start | bytes 6148 | tf_op jit(solution)/shard_map/while
  128.3 5.7 %copy-start.11 = (f32[512]{0:T(512)S(1)}, f32[512]{0:T(512)}, u32[]{:S(2)}) copy-start(f32[512]{0:T(512)} %get-tuple-element.1002) | copy-start | bytes 6148 | tf_op jit(solution)/shard_map/while
  128.3 5.7 %copy-start.14 = (f32[512]{0:T(512)S(1)}, f32[512]{0:T(512)}, u32[]{:S(2)}) copy-start(f32[512]{0:T(512)} %get-tuple-element.1038) | copy-start | bytes 6148 | tf_op jit(solution)/shard_map/while
  128.3 5.7 %copy-start.15 = (f32[1,512]{1,0:T(1,128)S(1)}, f32[1,512]{1,0:T(1,128)}, u32[]{:S(2)}) copy-start(f32[1,512]{1,0:T(1,128)} %get-tuple-element.1032) | copy-start | bytes 6148 | tf_op jit(solution)/shard_map/while
  139.1 5.7 %copy-start.5 = (f32[1,512]{1,0:T(1,128)S(1)}, f32[1,512]{1,0:T(1,128)}, u32[]{:S(2)}) copy-start(f32[1,512]{1,0:T(1,128)} %get-tuple-element.1028) | copy-start | bytes 6148 | tf_op jit(solution)/shard_map/while
  139.2 5.7 %copy-start.10 = (f32[512]{0:T(512)S(1)}, f32[512]{0:T(512)}, u32[]{:S(2)}) copy-start(f32[512]{0:T(512)} %get-tuple-element.1001) | copy-start | bytes 6148 | tf_op jit(solution)/shard_map/while
  139.2 5.7 %copy-start.11 = (f32[512]{0:T(512)S(1)}, f32[512]{0:T(512)}, u32[]{:S(2)}) copy-start(f32[512]{0:T(512)} %get-tuple-element.1002) | copy-start | bytes 6148 | tf_op jit(solution)/shard_map/while
  139.2 5.7 %copy-start.14 = (f32[512]{0:T(512)S(1)}, f32[512]{0:T(512)}, u32[]{:S(2)}) copy-start(f32[512]{0:T(512)} %get-tuple-element.1038) | copy-start | bytes 6148 | tf_op jit(solution)/shard_map/while
  139.2 5.7 %copy-start.15 = (f32[1,512]{1,0:T(1,128)S(1)}, f32[1,512]{1,0:T(1,128)}, u32[]{:S(2)}) copy-start(f32[1,512]{1,0:T(1,128)} %get-tuple-element.1032) | copy-start | bytes 6148 | tf_op jit(solution)/shard_map/while
  150.0 5.7 %copy-start.5 = (f32[1,512]{1,0:T(1,128)S(1)}, f32[1,512]{1,0:T(1,128)}, u32[]{:S(2)}) copy-start(f32[1,512]{1,0:T(1,128)} %get-tuple-element.1028) | copy-start | bytes 6148 | tf_op jit(solution)/shard_map/while
  150.0 5.7 %copy-start.10 = (f32[512]{0:T(512)S(1)}, f32[512]{0:T(512)}, u32[]{:S(2)}) copy-start(f32[512]{0:T(512)} %get-tuple-element.1001) | copy-start | bytes 6148 | tf_op jit(solution)/shard_map/while
  150.0 5.7 %copy-start.11 = (f32[512]{0:T(512)S(1)}, f32[512]{0:T(512)}, u32[]{:S(2)}) copy-start(f32[512]{0:T(512)} %get-tuple-element.1002) | copy-start | bytes 6148 | tf_op jit(solution)/shard_map/while
  150.0 5.7 %copy-start.14 = (f32[512]{0:T(512)S(1)}, f32[512]{0:T(512)}, u32[]{:S(2)}) copy-start(f32[512]{0:T(512)} %get-tuple-element.1038) | copy-start | bytes 6148 | tf_op jit(solution)/shard_map/while
  150.1 5.7 %copy-start.15 = (f32[1,512]{1,0:T(1,128)S(1)}, f32[1,512]{1,0:T(1,128)}, u32[]{:S(2)}) copy-start(f32[1,512]{1,0:T(1,128)} %get-tuple-element.1032) | copy-start | bytes 6148 | tf_op jit(solution)/shard_map/while
  160.9 5.7 %copy-start.5 = (f32[1,512]{1,0:T(1,128)S(1)}, f32[1,512]{1,0:T(1,128)}, u32[]{:S(2)}) copy-start(f32[1,512]{1,0:T(1,128)} %get-tuple-element.1028) | copy-start | bytes 6148 | tf_op jit(solution)/shard_map/while
  160.9 5.7 %copy-start.10 = (f32[512]{0:T(512)S(1)}, f32[512]{0:T(512)}, u32[]{:S(2)}) copy-start(f32[512]{0:T(512)} %get-tuple-element.1001) | copy-start | bytes 6148 | tf_op jit(solution)/shard_map/while
  160.9 5.7 %copy-start.11 = (f32[512]{0:T(512)S(1)}, f32[512]{0:T(512)}, u32[]{:S(2)}) copy-start(f32[512]{0:T(512)} %get-tuple-element.1002) | copy-start | bytes 6148 | tf_op jit(solution)/shard_map/while
  160.9 5.7 %copy-start.14 = (f32[512]{0:T(512)S(1)}, f32[512]{0:T(512)}, u32[]{:S(2)}) copy-start(f32[512]{0:T(512)} %get-tuple-element.1038) | copy-start | bytes 6148 | tf_op jit(solution)/shard_map/while
  160.9 5.7 %copy-start.15 = (f32[1,512]{1,0:T(1,128)S(1)}, f32[1,512]{1,0:T(1,128)}, u32[]{:S(2)}) copy-start(f32[1,512]{1,0:T(1,128)} %get-tuple-element.1032) | copy-start | bytes 6148 | tf_op jit(solution)/shard_map/while
  182.6 5.7 %copy-start.5 = (f32[1,512]{1,0:T(1,128)S(1)}, f32[1,512]{1,0:T(1,128)}, u32[]{:S(2)}) copy-start(f32[1,512]{1,0:T(1,128)} %get-tuple-element.1028) | copy-start | bytes 6148 | tf_op jit(solution)/shard_map/while
  182.6 5.7 %copy-start.10 = (f32[512]{0:T(512)S(1)}, f32[512]{0:T(512)}, u32[]{:S(2)}) copy-start(f32[512]{0:T(512)} %get-tuple-element.1001) | copy-start | bytes 6148 | tf_op jit(solution)/shard_map/while
  182.7 5.7 %copy-start.11 = (f32[512]{0:T(512)S(1)}, f32[512]{0:T(512)}, u32[]{:S(2)}) copy-start(f32[512]{0:T(512)} %get-tuple-element.1002) | copy-start | bytes 6148 | tf_op jit(solution)/shard_map/while
  182.7 5.7 %copy-start.14 = (f32[512]{0:T(512)S(1)}, f32[512]{0:T(512)}, u32[]{:S(2)}) copy-start(f32[512]{0:T(512)} %get-tuple-element.1038) | copy-start | bytes 6148 | tf_op jit(solution)/shard_map/while
  182.7 5.7 %copy-start.15 = (f32[1,512]{1,0:T(1,128)S(1)}, f32[1,512]{1,0:T(1,128)}, u32[]{:S(2)}) copy-start(f32[1,512]{1,0:T(1,128)} %get-tuple-element.1032) | copy-start | bytes 6148 | tf_op jit(solution)/shard_map/while
  280.2 61.5 %copy-start.6 = (f32[512]{0:T(512)S(1)}, f32[512]{0:T(512)}, u32[]{:S(2)}) copy-start(f32[512]{0:T(512)} %custom-call) | copy-start | bytes 6148
  280.2 61.5 %copy-start.7 = (f32[512]{0:T(512)S(1)}, f32[512]{0:T(512)}, u32[]{:S(2)}) copy-start(f32[512]{0:T(512)} %custom-call.1) | copy-start | bytes 6148
  353.2 11.3 %copy-start.13 = (f32[512]{0:T(512)S(1)}, f32[512]{0:T(512)}, u32[]{:S(2)}) copy-start(f32[512]{0:T(512)} %param.22) | copy-start | bytes 6148
  (60 other events, 335.7 us)
Sparse Core Ops, SparseCore 0:
  11.0 89.7 all-gather.3
where the time goes:
time: 378 us; the launch traced here: 373 us
  matrix products  134 us (35%)
  waiting for transfers between devices  85.1 us (23%)
  blocking collectives  69.5 us (18%)
  local copies, waits for them, and re-layouts  43.1 us (11%)
  other arithmetic  22.5 us (6%)
  between operations  13.7 us (4%)
  loops' own time  5.22 us (1%)
    all_gather x1, waiting for transfers between devices, on_device(): lax.all_gather(normed, 'tp', axis=0, tiled=True)  85.1 us
    all_gather x1, blocking collectives, gathered_once(): both, at, found = (lax.all_gather(jnp.concatenate(lines), axis), 0, {})  60.4 us
    dot_general x16, matrix products, advance(): acc_im = jnp.dot(lower, w_im, precision=HIGHEST)  48.1 us
    dot_general x16, matrix products, advance(): acc_re = jnp.dot(lower, w_re, precision=HIGHEST)  32.4 us
    slice x32, local copies, waits for them, and re-layouts, advance(): ends = (cum_re[-1], cum_im[-1], full_re[-1], full_im[-1])  18.8 us
    dot_general x16, matrix products, advance(): in_im = jnp.dot(grouped, push_im, precision=HIGHEST)  15.3 us
    dot_general x16, matrix products, advance(): in_re = jnp.dot(grouped, push_re, precision=HIGHEST)  15.3 us
    dot_general x16, matrix products, advance(): elapsed = jnp.dot(lower, time_part, precision=HIGHEST)[:, None]  13.3 us
  transfers between devices with their start and end apart: 1, of which 1 were waited for; matrix products, arithmetic and copies ran while one was open for 1% of the time, Pallas kernels for 0%

commit v1 on v0

--- a/solution.py
+++ b/solution.py
@@ -6,6 +6,11 @@
 
 SPAN = 64
 HIGHEST = lax.Precision.HIGHEST
+
+
+def gather_by_exchange(value, axis, dim):
+    copies = jnp.concatenate([value] * lax.axis_size(axis), axis=dim)
+    return lax.all_to_all(copies, axis, dim, dim, tiled=True)
 
 
 def gathered_once(array, axis):
@@ -124,9 +129,7 @@
     normed = rms_rows(tokens, in_gain)
     rates, freqs, maps, reads = (decay_rate, frequency, input_map, readout)
     drive = jnp.dot(
-        lax.all_gather(normed, "tp", axis=0, tiled=True),
-        in_proj,
-        preferred_element_type=jnp.float32,
+        gather_by_exchange(normed, "tp", 0), in_proj, preferred_element_type=jnp.float32
     ).astype(jnp.bfloat16)
     tables = block_tables(maps, reads)
     flat_rates = rates.reshape(-1)

time: 378 us -> 367 us (0.971)
  waiting for transfers between devices: 85.1 us -> 22.5 us
  blocking collectives: 69.5 us -> 129 us
  between operations: 13.7 us -> 0.25 us
  starting transfers between devices: 0.06 us -> 5.26 us
    all_gather x1 -> x0, waiting for transfers between devices: 85.1 us -> none  [on_device(): lax.all_gather(normed, 'tp', axis=0, tiled=True)]
    all_gather x1, blocking collectives: 60.4 us -> 120 us  [gathered_once(): both, at, found = (lax.all_gather(jnp.concatenate(lines), axis), 0, {})]
    all_to_all x0 -> x1, waiting for transfers between devices: none -> 22.5 us  [gather_by_exchange(): return lax.all_to_all(copies, axis, dim, dim, tiled=True)]
    all_to_all x0 -> x1, starting transfers between devices: none -> 5.26 us  [gather_by_exchange(): return lax.all_to_all(copies, axis, dim, dim, tiled=True)]
where the time goes in v1:
time: 367 us; the launch traced here: 362 us
  matrix products  134 us (37%)
  blocking collectives  129 us (35%)
  local copies, waits for them, and re-layouts  42.6 us (12%)
  other arithmetic  23.8 us (6%)
  waiting for transfers between devices  22.5 us (6%)
  starting transfers between devices  5.26 us (1%)
  loops' own time  5.22 us (1%)
    all_gather x1, blocking collectives, gathered_once(): both, at, found = (lax.all_gather(jnp.concatenate(lines), axis), 0, {})  120 us
    dot_general x16, matrix products, advance(): acc_im = jnp.dot(lower, w_im, precision=HIGHEST)  47.9 us
    dot_general x16, matrix products, advance(): acc_re = jnp.dot(lower, w_re, precision=HIGHEST)  32.6 us
    all_to_all x1, waiting for transfers between devices, gather_by_exchange(): return lax.all_to_all(copies, axis, dim, dim, tiled=True)  22.5 us
    slice x32, local copies, waits for them, and re-layouts, advance(): ends = (cum_re[-1], cum_im[-1], full_re[-1], full_im[-1])  18.5 us
    dot_general x16, matrix products, advance(): in_re = jnp.dot(grouped, push_re, precision=HIGHEST)  15.3 us
    dot_general x16, matrix products, advance(): in_im = jnp.dot(grouped, push_im, precision=HIGHEST)  15.3 us
    dot_general x16, matrix products, advance(): elapsed = jnp.dot(lower, time_part, precision=HIGHEST)[:, None]  13.1 us
  transfers between devices with their start and end apart: 1, of which 1 were waited for; matrix products, arithmetic and copies ran while one was open for 1% of the time, Pallas kernels for 0%

profile of v1, /device:TPU:33, one launch (start us, length us, event | category | flops | bytes accessed | tf_op | source)
XLA Modules:
  0.0 362.5 jit_solution(3971909153354711741)
XLA Ops:
  3.2 2.3 pad_maximum_fusion
  5.5 5.3 %all-to-all-start = ((bf16[4,256,2048]{2,1,0:T(8,128)(2,1)}), bf16[4,256,2048]{2,1,0:T(8,128)(2,1)}, u32[]{:S(2)}, u32[]{:S(2)}) async-start(bf16[4,256,2048]{2,1,0:T(8,128)(2,1)} %bitcast.149), calls=%async_computation | async-start | bytes 8388608 | tf_op jit(solution)/shard_map/all_to_all | solution.py:13
  15.6 22.5 %all-to-all-done = bf16[4,256,2048]{2,1,0:T(8,128)(2,1)} async-done(((bf16[4,256,2048]{2,1,0:T(8,128)(2,1)}), bf16[4,256,2048]{2,1,0:T(8,128)(2,1)}, u32[]{:S(2)}, u32[]{:S(2)}) %all-to-all-start) | async-done | bytes 4194336 | tf_op jit(solution)/shard_map/all_to_all | solution.py:13
  38.1 4.3 %convolution_convert_fusion.1 = bf16[1024,128]{1,0:T(8,128)(2,1)} fusion(bf16[1024,2048]{1,0:T(8,128)(2,1)} %bitcast.1, bf16[2048,128]{1,0:T(8,128)(2,1)} %param.17), kind=kOutput, calls=%fused_computation.82 | convolution fusion | flops 537001984 | bytes 4980736 | tf_op jit(solution)/shard_map/dot_general | solution.py:131
  43.5 173.4 %while.48 = (s32[]{:T(128)}, f32[512]{0:T(512)S(1)}, f32[512]{0:T(512)S(1)}, f32[512]{0:T(512)}, f32[512]{0:T(512)}, /*index=5*/f32[16,64,512]{2,1,0:T(8,128)}, ...) while((s32[]{:T(128)}, f32[512]{0:T(512)S(1)}, ...), condition=%wide.wide.region_2.3_spmd.clone.clone.clone, body=%wide.wide.region_1.2_spmd.clone.clone.clone.sunk | while | flops 153889792 | bytes 4405837 | solution.py:148
  47.5 2.0 convolution_bitcast_fusion.8
  49.6 3.0 add_dynamic-update-slice_fusion.3
  58.3 2.0 convolution_bitcast_fusion.8
  60.4 3.0 add_dynamic-update-slice_fusion.3
  71.2 3.0 add_dynamic-update-slice_fusion.3
  82.1 3.0 add_dynamic-update-slice_fusion.3
  90.8 2.0 convolution_bitcast_fusion.8
  92.9 3.0 add_dynamic-update-slice_fusion.3
  103.7 3.0 add_dynamic-update-slice_fusion.3
  114.6 3.0 add_dynamic-update-slice_fusion.3
  123.3 2.0 convolution_bitcast_fusion.8
  125.4 3.0 add_dynamic-update-slice_fusion.3
  136.2 3.0 add_dynamic-update-slice_fusion.3
  147.1 3.0 add_dynamic-update-slice_fusion.3
  157.9 3.0 add_dynamic-update-slice_fusion.3
  166.6 2.0 convolution_bitcast_fusion.8
  168.8 3.0 add_dynamic-update-slice_fusion.3
  177.5 2.0 convolution_bitcast_fusion.8
  179.6 3.0 add_dynamic-update-slice_fusion.3
  190.4 3.0 add_dynamic-update-slice_fusion.3
  201.3 3.0 add_dynamic-update-slice_fusion.3
  210.0 2.0 convolution_bitcast_fusion.8
  212.1 3.0 add_dynamic-update-slice_fusion.3
  217.6 120.1 %all-gather.1 = f32[64,4,512]{2,1,0:T(4,128)S(1)} all-gather(f32[1,4,512]{2,1,0:T(4,128)S(1)} %maximum_bitcast_fusion), channel_id=2, replica_groups=mesh['grp'=2,'sp'=64,'tp'=4] {'sp'}, dimensions={0}, use_global_device_ids=true | all-gather | bytes 532480 | tf_op jit(solution)/shard_map/all_gather | solution.py:24
  338.1 5.1 %while.47 = (s32[]{:T(128)}, f32[512]{0:T(512)S(1)}, f32[512]{0:T(512)S(1)}, s32[]{:T(128)}, f32[64,512]{1,0:T(8,128)S(1)}, /*index=5*/f32[64,512]{1,0:T(8,128)S...) while((s32[]{:T(128)}, f32[512]{0:T(512)S(1)}, f32[512]{0:T(512)S(1)}, ...), condition=%wide.region_4.5_spmd.clone, body=%wide.region_3.4_spmd.clone.sunk | while | flops 6148 | bytes 32897 | solution.py:44
  343.3 4.6 %multiply_add_fusion.5 = (f32[16,64,512]{2,1,0:T(8,128)S(1)}, f32[16,64,512]{2,1,0:T(8,128)S(1)}) fusion(f32[16,64,512]{2,1,0:T(8,128)} %get-tuple-element.435, f32[16,64,512]{2,1,0:T(8,128)} %get-tuple-element.437, f32[16,64,512]{2,1,0:T(8,128)} %get-tuple-element.429, f32[512]{0:T(512)S(1)} %get-tuple-element.436, f32[512]{0:T(512)S(1)} %get-tuple-element.434, ...), kind=kLoop, calls=%fused_computation.79 | loop fusion | flops 4194304 | bytes 12587008 | tf_op jit(solution)/shard_map/add | solution.py:161
  351.7 8.9 %all_to_all.25 = bf16[4,256,128]{1,2,0:T(8,128)(2,1)S(1)} all-to-all(bf16[4,256,128]{1,2,0:T(8,128)(2,1)S(1)} %copy.20), channel_id=1, replica_groups=mesh['grp'=2,'sp'=64,'tp'=4] {'tp'}, dimensions={0} | all-to-all | bytes 524288 | tf_op jit(solution)/shard_map/all_to_all | solution.py:163
  (627 shorter events, 127.0 us)
Async XLA Ops:
  0.0 360.8 %copy-start = (bf16[512,2048]{1,0:T(8,128)(2,1)S(1)}, bf16[512,2048]{1,0:T(8,128)(2,1)}, u32[]{:S(2)}) copy-start(bf16[512,2048]{1,0:T(8,128)(2,1)} %param.23) | copy-start | bytes 6291460
  5.5 7.3 %copy-start.12 = (f32[1024]{0:T(1024)S(1)}, f32[1024]{0:T(1024)}, u32[]{:S(2)}) copy-start(f32[1024]{0:T(1024)} %param.15) | copy-start | bytes 12292
  5.5 8.0 %copy-start.3 = (f32[2,8,16,64]{3,2,1,0:T(8,128)S(1)}, f32[2,8,16,64]{3,2,1,0:T(8,128)}, u32[]{:S(2)}) copy-start(f32[2,8,16,64]{3,2,1,0:T(8,128)} %param.21) | copy-start | bytes 196612
  5.5 32.6 %all-to-all-start = ((bf16[4,256,2048]{2,1,0:T(8,128)(2,1)}), bf16[4,256,2048]{2,1,0:T(8,128)(2,1)}, u32[]{:S(2)}, u32[]{:S(2)}) async-start(bf16[4,256,2048]{2,1,0:T(8,128)(2,1)} %bitcast.149), calls=%async_computation | async-start | bytes 8388608 | tf_op jit(solution)/shard_map/all_to_all | solution.py:13
  163.0 5.7 %copy-start.5 = (f32[1,512]{1,0:T(1,128)S(1)}, f32[1,512]{1,0:T(1,128)}, u32[]{:S(2)}) copy-start(f32[1,512]{1,0:T(1,128)} %get-tuple-element.1028) | copy-start | bytes 6148 | tf_op jit(solution)/shard_map/while
  163.0 5.7 %copy-start.10 = (f32[512]{0:T(512)S(1)}, f32[512]{0:T(512)}, u32[]{:S(2)}) copy-start(f32[512]{0:T(512)} %get-tuple-element.1001) | copy-start | bytes 6148 | tf_op jit(solution)/shard_map/while
  163.0 5.7 %copy-start.11 = (f32[512]{0:T(512)S(1)}, f32[512]{0:T(512)}, u32[]{:S(2)}) copy-start(f32[512]{0:T(512)} %get-tuple-element.1002) | copy-start | bytes 6148 | tf_op jit(solution)/shard_map/while
  163.0 5.7 %copy-start.14 = (f32[512]{0:T(512)S(1)}, f32[512]{0:T(512)}, u32[]{:S(2)}) copy-start(f32[512]{0:T(512)} %get-tuple-element.1038) | copy-start | bytes 6148 | tf_op jit(solution)/shard_map/while
  163.0 5.7 %copy-start.15 = (f32[1,512]{1,0:T(1,128)S(1)}, f32[1,512]{1,0:T(1,128)}, u32[]{:S(2)}) copy-start(f32[1,512]{1,0:T(1,128)} %get-tuple-element.1032) | copy-start | bytes 6148 | tf_op jit(solution)/shard_map/while
  173.8 5.7 %copy-start.5 = (f32[1,512]{1,0:T(1,128)S(1)}, f32[1,512]{1,0:T(1,128)}, u32[]{:S(2)}) copy-start(f32[1,512]{1,0:T(1,128)} %get-tuple-element.1028) | copy-start | bytes 6148 | tf_op jit(solution)/shard_map/while
  173.8 5.7 %copy-start.10 = (f32[512]{0:T(512)S(1)}, f32[512]{0:T(512)}, u32[]{:S(2)}) copy-start(f32[512]{0:T(512)} %get-tuple-element.1001) | copy-start | bytes 6148 | tf_op jit(solution)/shard_map/while
  173.9 5.7 %copy-start.11 = (f32[512]{0:T(512)S(1)}, f32[512]{0:T(512)}, u32[]{:S(2)}) copy-start(f32[512]{0:T(512)} %get-tuple-element.1002) | copy-start | bytes 6148 | tf_op jit(solution)/shard_map/while
  173.9 5.7 %copy-start.14 = (f32[512]{0:T(512)S(1)}, f32[512]{0:T(512)}, u32[]{:S(2)}) copy-start(f32[512]{0:T(512)} %get-tuple-element.1038) | copy-start | bytes 6148 | tf_op jit(solution)/shard_map/while
  173.9 5.7 %copy-start.15 = (f32[1,512]{1,0:T(1,128)S(1)}, f32[1,512]{1,0:T(1,128)}, u32[]{:S(2)}) copy-start(f32[1,512]{1,0:T(1,128)} %get-tuple-element.1032) | copy-start | bytes 6148 | tf_op jit(solution)/shard_map/while
  184.7 5.7 %copy-start.5 = (f32[1,512]{1,0:T(1,128)S(1)}, f32[1,512]{1,0:T(1,128)}, u32[]{:S(2)}) copy-start(f32[1,512]{1,0:T(1,128)} %get-tuple-element.1028) | copy-start | bytes 6148 | tf_op jit(solution)/shard_map/while
  184.7 5.7 %copy-start.10 = (f32[512]{0:T(512)S(1)}, f32[512]{0:T(512)}, u32[]{:S(2)}) copy-start(f32[512]{0:T(512)} %get-tuple-element.1001) | copy-start | bytes 6148 | tf_op jit(solution)/shard_map/while
  184.7 5.7 %copy-start.11 = (f32[512]{0:T(512)S(1)}, f32[512]{0:T(512)}, u32[]{:S(2)}) copy-start(f32[512]{0:T(512)} %get-tuple-element.1002) | copy-start | bytes 6148 | tf_op jit(solution)/shard_map/while
  184.7 5.7 %copy-start.14 = (f32[512]{0:T(512)S(1)}, f32[512]{0:T(512)}, u32[]{:S(2)}) copy-start(f32[512]{0:T(512)} %get-tuple-element.1038) | copy-start | bytes 6148 | tf_op jit(solution)/shard_map/while
  184.7 5.7 %copy-start.15 = (f32[1,512]{1,0:T(1,128)S(1)}, f32[1,512]{1,0:T(1,128)}, u32[]{:S(2)}) copy-start(f32[1,512]{1,0:T(1,128)} %get-tuple-element.1032) | copy-start | bytes 6148 | tf_op jit(solution)/shard_map/while
  195.5 5.7 %copy-start.5 = (f32[1,512]{1,0:T(1,128)S(1)}, f32[1,512]{1,0:T(1,128)}, u32[]{:S(2)}) copy-start(f32[1,512]{1,0:T(1,128)} %get-tuple-element.1028) | copy-start | bytes 6148 | tf_op jit(solution)/shard_map/while
  195.5 5.7 %copy-start.10 = (f32[512]{0:T(512)S(1)}, f32[512]{0:T(512)}, u32[]{:S(2)}) copy-start(f32[512]{0:T(512)} %get-tuple-element.1001) | copy-start | bytes 6148 | tf_op jit(solution)/shard_map/while
  195.5 5.7 %copy-start.11 = (f32[512]{0:T(512)S(1)}, f32[512]{0:T(512)}, u32[]{:S(2)}) copy-start(f32[512]{0:T(512)} %get-tuple-element.1002) | copy-start | bytes 6148 | tf_op jit(solution)/shard_map/while
  195.5 5.7 %copy-start.14 = (f32[512]{0:T(512)S(1)}, f32[512]{0:T(512)}, u32[]{:S(2)}) copy-start(f32[512]{0:T(512)} %get-tuple-element.1038) | copy-start | bytes 6148 | tf_op jit(solution)/shard_map/while
  195.5 5.7 %copy-start.15 = (f32[1,512]{1,0:T(1,128)S(1)}, f32[1,512]{1,0:T(1,128)}, u32[]{:S(2)}) copy-start(f32[1,512]{1,0:T(1,128)} %get-tuple-element.1032) | copy-start | bytes 6148 | tf_op jit(solution)/shard_map/while
  206.3 5.7 %copy-start.5 = (f32[1,512]{1,0:T(1,128)S(1)}, f32[1,512]{1,0:T(1,128)}, u32[]{:S(2)}) copy-start(f32[1,512]{1,0:T(1,128)} %get-tuple-element.1028) | copy-start | bytes 6148 | tf_op jit(solution)/shard_map/while
  206.4 5.7 %copy-start.10 = (f32[512]{0:T(512)S(1)}, f32[512]{0:T(512)}, u32[]{:S(2)}) copy-start(f32[512]{0:T(512)} %get-tuple-element.1001) | copy-start | bytes 6148 | tf_op jit(solution)/shard_map/while
  206.4 5.7 %copy-start.11 = (f32[512]{0:T(512)S(1)}, f32[512]{0:T(512)}, u32[]{:S(2)}) copy-start(f32[512]{0:T(512)} %get-tuple-element.1002) | copy-start | bytes 6148 | tf_op jit(solution)/shard_map/while
  206.4 5.7 %copy-start.14 = (f32[512]{0:T(512)S(1)}, f32[512]{0:T(512)}, u32[]{:S(2)}) copy-start(f32[512]{0:T(512)} %get-tuple-element.1038) | copy-start | bytes 6148 | tf_op jit(solution)/shard_map/while
  206.4 5.7 %copy-start.15 = (f32[1,512]{1,0:T(1,128)S(1)}, f32[1,512]{1,0:T(1,128)}, u32[]{:S(2)}) copy-start(f32[1,512]{1,0:T(1,128)} %get-tuple-element.1032) | copy-start | bytes 6148 | tf_op jit(solution)/shard_map/while
  216.9 121.2 %copy-start.6 = (f32[512]{0:T(512)S(1)}, f32[512]{0:T(512)}, u32[]{:S(2)}) copy-start(f32[512]{0:T(512)} %custom-call) | copy-start | bytes 6148
  216.9 121.2 %copy-start.7 = (f32[512]{0:T(512)S(1)}, f32[512]{0:T(512)}, u32[]{:S(2)}) copy-start(f32[512]{0:T(512)} %custom-call.1) | copy-start | bytes 6148
  349.7 11.0 %copy-start.13 = (f32[512]{0:T(512)S(1)}, f32[512]{0:T(512)}, u32[]{:S(2)}) copy-start(f32[512]{0:T(512)} %param.22) | copy-start | bytes 6148
  (60 other events, 336.8 us)
